TPU v7x, 32 devices: a whole 2x2x4 slice. The times are simulated.
32 devices in a mesh: sp: 4 (over y, x), tp: 8 (over z, core).
Axes of the slice: x: 2, y: 2, z: 4, core: 2. Of those that a mesh axis runs over, the one named last changes fastest.
Arguments:
- tokens: bfloat16 [2048, 2048], P(('sp', 'tp')), may hold values from -6 to 6
- query_vectors: bfloat16 [2048, 2048], P('sp', 'tp'), may hold values from -8 to 8
- key_vectors: bfloat16 [2048, 2048], P('sp', 'tp'), may hold values from -8 to 8
- value_vectors: bfloat16 [2048, 2048], P('sp', 'tp'), may hold values from -24 to 24
- cum_gate: float32 [2048, 32], P('sp', 'tp'), may hold values from -260 to 0, as said below
- out_weight: bfloat16 [2048, 2048], P('tp'), may hold values from -0.125 to 0.125
- norm_gain: float32 [2048], replicated, may hold values from 0.1 to 1.9
- gate_weight: bfloat16 [4, 2048, 7168], P('sp', None, 'tp'), may hold values from -0.125 to 0.125
- up_weight: bfloat16 [4, 2048, 7168], P('sp', None, 'tp'), may hold values from -0.125 to 0.125
- down_weight: bfloat16 [4, 7168, 2048], P('sp', 'tp'), may hold values from -0.0625 to 0.0625
- expert_ids: int32 [2048, 2], P(('sp', 'tp')), may hold values from 0 to 3, all different within a row; in each aligned block of 64 rows (0 to 63, 64 to 127, ...) at most 48 rows name the same one
- route_weights: float32 [2048, 2], P(('sp', 'tp')), may hold values from 0.2 to 1
Outputs:
- layer_output: bfloat16 [2048, 2048], P(('sp', 'tp'))
Inputs may be any that keep to these rules, and one draw needn't show every extreme that they name: `cum_gate`: along the positions each head's values never rise. `expert_ids`: within the rows of one device no expert is named by more than 48 rows, and in some devices' rows one expert is named by exactly 48; a row names 2 different experts.
All inputs are finite; a program needn't handle non-finite values.
Results may differ from a plain program's by a relative error of at most 0.014.
Values may be sent and summed in bfloat16 or wider, within the bound.
A program may use at most 128 MiB of HBM per device.

v0:
```python
import functools
import math

import jax
import jax.numpy as jnp
from jax import lax
from jax.experimental import pallas as pl
from jax.experimental.pallas import tpu as pltpu
from jax.sharding import PartitionSpec as P

MESH = pl.DeviceIdType.MESH
VMEM_LIMIT = 60 * 1024 * 1024
F32 = jnp.float32
BF16 = jnp.bfloat16


def rcopy(src, dst, ssem, rsem, where):
    return pltpu.make_async_remote_copy(
        src_ref=src, dst_ref=dst, send_sem=ssem, recv_sem=rsem, device_id=where, device_id_type=MESH
    )


def vmem_specs(count):
    return [pl.BlockSpec(memory_space=pltpu.VMEM)] * count


def attend_kernel(sp, heads, q, k, v, g, w, out, ka, va, ga, att, top_s, sum_s, acc_s, ssem, rsem):
    s = lax.axis_index("sp")
    barrier = pltpu.get_barrier_semaphore()
    for d in range(1, sp):
        pl.semaphore_signal(barrier, inc=1, device_id={"sp": lax.rem(s + d, sp)}, device_id_type=MESH)
    pl.semaphore_wait(barrier, sp - 1)
    pairs = ((k, ka), (v, va), (g, ga))

    def copy(n, d):
        src, dst = pairs[n]
        return rcopy(src, dst.at[d], ssem.at[n, d], rsem.at[n, d], {"sp": lax.rem(s + d, sp)})

    for d in range(1, sp):

        @pl.when(s + d < sp)
        def _():
            for n in range(3):
                copy(n, d).start()

    rows, width = q.shape
    hd = width // heads
    tile = math.gcd(rows, 256)
    log2e = 1.4426950408889634
    coef = hd ** (-0.5) * log2e
    units = [(h, i) for h in range(heads) for i in range(rows // tile)]

    def scores(h, i, kb, gb):
        qt = q[i * tile : (i + 1) * tile, h * hd : (h + 1) * hd]
        return (
            lax.dot_general(qt, kb, (((1,), (1,)), ((), ())), preferred_element_type=F32) * coef
            - gb * log2e
        )

    for h, i in units:
        cols = slice(h * hd, (h + 1) * hd)
        seen = (i + 1) * tile
        sc = scores(h, i, k[0:seen, cols], g[h : h + 1, 0:seen])
        row = lax.broadcasted_iota(jnp.int32, sc.shape, 0) + i * tile
        col = lax.broadcasted_iota(jnp.int32, sc.shape, 1)
        sc = jnp.where(col <= row, sc, -1e30)
        peak = jnp.max(sc, axis=1, keepdims=True)
        ex = jnp.exp2(sc - peak)
        at = slice(i * tile, seen)
        top_s[h, at] = peak
        sum_s[h, at] = jnp.sum(ex, axis=1, keepdims=True)
        acc_s[h, at] = jnp.dot(ex.astype(BF16), v[0:seen, cols], preferred_element_type=F32)

    def step(d, _):
        for n in range(3):
            copy(n, d).wait_recv()
        for h, i in units:
            cols = slice(h * hd, (h + 1) * hd)
            at = slice(i * tile, (i + 1) * tile)
            sc = scores(h, i, ka[d, :, cols], ga[d, h : h + 1, :])
            peak = top_s[h, at]
            new = jnp.maximum(peak, jnp.max(sc, axis=1, keepdims=True))
            ex = jnp.exp2(sc - new)
            fix = jnp.exp2(peak - new)
            top_s[h, at] = new
            sum_s[h, at] = sum_s[h, at] * fix + jnp.sum(ex, axis=1, keepdims=True)
            acc_s[h, at] = acc_s[h, at] * fix + jnp.dot(
                ex.astype(BF16), va[d, :, cols], preferred_element_type=F32
            )
        return 0

    lax.fori_loop(1, s + 1, step, 0)
    for h, i in units:
        at = slice(i * tile, (i + 1) * tile)
        att[at, h * hd : (h + 1) * hd] = (acc_s[h, at] / sum_s[h, at]).astype(BF16)
    wide = w.shape[1]
    chunk = math.gcd(wide, 512)
    for n in range(wide // chunk):
        cut = slice(n * chunk, (n + 1) * chunk)
        out[:, cut] = jnp.dot(att[...], w[:, cut], preferred_element_type=F32).astype(BF16)
    for d in range(1, sp):

        @pl.when(s + d < sp)
        def _():
            for n in range(3):
                copy(n, d).wait_send()


def greet(sp, zn, s, z, c, partner):
    barrier = pltpu.get_barrier_semaphore()
    pl.semaphore_signal(barrier, inc=1, device_id={"tp": partner}, device_id_type=MESH)
    for i in range(1, zn):
        pl.semaphore_signal(
            barrier, inc=1, device_id={"tp": 2 * lax.rem(z + i, zn) + c}, device_id_type=MESH
        )
    for d in range(1, sp):
        pl.semaphore_signal(barrier, inc=1, device_id={"sp": lax.rem(s + d, sp)}, device_id_type=MESH)
    pl.semaphore_wait(barrier, 1 + (zn - 1) + (sp - 1))


def experts_kernel(
    sp, zn, p, tok, gain, place, comb, wg_in, wu_in, wd_in, out,
    wg, wu, wd, xr, cb, zr, ng, pg, combs, db, rows, hid, y, pr, cs, eb, mb, rr, keep,
    ws, xs, xrs, as_, ars, zs, zrs, ns, nrs, ds_, drs, fs, frs, ps, prs, es, ers, ms, mrs,
):
    s, t = lax.axis_index("sp"), lax.axis_index("tp")
    z, c = t // 2, lax.rem(t, 2)
    partner = t + 1 - 2 * c
    T, D = tok.shape
    cap = rows.shape[3]
    loads = [
        pltpu.make_async_copy(a.at[0], b, ws.at[n])
        for n, (a, b) in enumerate(((wg_in, wg), (wu_in, wu), (wd_in, wd)))
    ]
    for load in loads:
        load.start()
    greet(sp, zn, s, z, c, partner)
    offs = [0] + sorted(range(1, zn), key=lambda i: -min(i, zn - i))
    outs = offs[1:] + [0]

    def at_z(i):
        return 2 * lax.rem(z + i, zn) + c

    def peer(d):
        return lax.rem(s + d, sp)

    def behind(d):
        return lax.rem(s + sp - d, sp)

    def swap(i):
        zz = lax.rem(z + outs[i], zn)
        src = p.at[pl.ds(pl.multiple_of((2 * zz + 1 - c) * T, 16), T)]
        return rcopy(src, xr.at[i], xs.at[i], xrs.at[i], {"tp": partner})

    def aux(n, i):
        src, dst = ((place, pg), (comb, combs))[n]
        return rcopy(src, dst.at[i], as_.at[n, i], ars.at[n, i], {"tp": at_z(offs[i])})

    def reduce_to(i):
        return rcopy(cb.at[i], zr.at[i], zs.at[i], zrs.at[i], {"tp": at_z(outs[i])})

    def spread(i):
        return rcopy(ng.at[0], ng.at[i], ns.at[i], nrs.at[i], {"tp": at_z(offs[i])})

    def route(i, d):
        return rcopy(
            db.at[i, peer(d)], rows.at[i, s, c], ds_.at[i, d], drs.at[i, d], {"sp": peer(d)}
        )

    def routed(i, d):
        return rcopy(
            db.at[i, peer(d)], rows.at[i, behind(d), c], ds_.at[i, d], drs.at[i, d], {"sp": peer(d)}
        )

    def forward(i, d):
        ref = rows.at[i, behind(d), c]
        return rcopy(ref, ref, fs.at[i, d], frs.at[i, d], {"tp": partner})

    def forwarded(i, d):
        ref = rows.at[i, behind(d), 1 - c]
        return rcopy(ref, ref, fs.at[i, d], frs.at[i, d], {"tp": partner})

    def swap_out(i, d):
        return rcopy(y.at[i, peer(d), 1 - c], pr.at[i, d], ps.at[i, d], prs.at[i, d], {"tp": partner})

    def back(i, d, slot):
        return rcopy(cs.at[i, d], eb.at[i, slot], es.at[i, d], ers.at[i, d], {"sp": peer(d)})

    def reduce_out(i):
        return rcopy(
            mb.at[i], rr.at[i], ms.at[i], mrs.at[i], {"tp": at_z(zn - offs[i])}
        )

    def dispatch(i):
        if i > 0:
            aux(0, i).wait_recv()
            spread(i).wait_recv()
        moved = jnp.dot(pg[i], ng[i], preferred_element_type=F32)
        for e in range(sp):
            db[i, e] = moved[e * cap : (e + 1) * cap].astype(BF16)
        for d in range(1, sp):
            route(i, d).start()
        rows[i, s, c] = db[i, s]
        forward(i, 0).start()

    def pass_on(i):
        def arrive(d, _):
            routed(i, d).wait_recv()
            forward(i, d).start()
            return 0

        lax.fori_loop(1, sp, arrive, 0)

    def each(count, body):
        if count * rows.shape[1] <= 64:
            for n in range(count):
                body(n)
        else:
            lax.fori_loop(0, count, lambda n, _: (body(n), 0)[1], 0)

    def expert(i):
        def landed(d, _):
            forwarded(i, d).wait_recv()
            return 0

        lax.fori_loop(0, sp, landed, 0)
        x = rows.at[i]
        many = sp * 2 * cap
        units = wg.shape[1]
        step = 256

        def into(start, size):
            cut = pl.ds(start, size)
            xv = x[...].reshape(many, D)
            gate = jnp.dot(xv, wg[:, cut], preferred_element_type=F32)
            up = jnp.dot(xv, wu[:, cut], preferred_element_type=F32)
            hid[:, cut] = (gate / (1.0 + jnp.exp(-gate)) * up).astype(BF16)

        each(units // step, lambda n: into(pl.multiple_of(n * step, step), step))
        if units % step:
            into(units - units % step, units % step)
        chunk = math.gcd(D, 512)

        def down(n):
            cut = pl.ds(pl.multiple_of(n * chunk, chunk), chunk)
            got = jnp.dot(hid[...], wd[:, cut], preferred_element_type=F32).astype(BF16)
            y[i, :, :, :, cut] = got.reshape(sp, 2, cap, chunk)

        each(D // chunk, down)
        for d in list(range(1, sp)) + [0]:
            swap_out(i, d).start()

    def give_back(i):
        def both(d):
            swap_out(i, d).wait_recv()
            return (y[i, peer(d), c].astype(F32) + pr[i, d].astype(F32)).astype(BF16)

        def send(d, _):
            cs[i, d] = both(d)
            back(i, d, s).start()
            return 0

        lax.fori_loop(1, sp, send, 0)
        eb[i, s] = both(0)

    def mix(i):
        if i > 0:
            aux(1, i).wait_recv()
        for d in range(1, sp):
            back(i, d, behind(d)).wait_recv()
        mixed = jnp.dot(combs[i], eb[i].reshape(sp * cap, D), preferred_element_type=F32)
        mixed = mixed[0:T] + mixed[T : 2 * T]
        if i > 0:
            mb[i] = mixed.astype(BF16)
            reduce_out(i).start()
        else:
            keep[...] = mixed

    for i in range(zn):
        swap(i).start()
    for i in range(1, zn):
        for n in range(2):
            aux(n, i).start()
    pg[0] = place[...]
    combs[0] = comb[...]
    own = None
    for i in range(zn):
        swap(i).wait_recv()
        zz = lax.rem(z + outs[i], zn)
        both = p[pl.ds(pl.multiple_of((2 * zz + c) * T, 16), T), :].astype(F32) + xr[i].astype(F32)
        if i < zn - 1:
            cb[i] = both.astype(BF16)
            reduce_to(i).start()
        else:
            own = both
    for i in range(zn - 1):
        reduce_to(i).wait_recv()
        own = own + zr[i].astype(F32)
    st = (tok[...].astype(F32) + own).astype(BF16)
    out[...] = st
    wide = st.astype(F32)
    inverse = lax.rsqrt(jnp.mean(wide * wide, axis=1, keepdims=True) + 1e-05)
    ng[0] = (wide * inverse * gain[...]).astype(BF16)
    for i in range(1, zn):
        spread(i).start()
    dispatch(0)
    if zn > 1:
        dispatch(1)
    for load in loads:
        load.wait()
    for i in range(zn):
        pass_on(i)
        if i + 2 < zn:
            dispatch(i + 2)
        expert(i)
        if i >= 1:
            give_back(i - 1)
        if i >= 2:
            mix(i - 2)
    give_back(zn - 1)
    if zn > 1:
        mix(zn - 2)
    mix(zn - 1)
    total = out[...].astype(F32) + keep[...]
    for i in range(1, zn):
        reduce_out(i).wait_recv()
        total = total + rr[i].astype(F32)
    out[...] = total.astype(BF16)
    for i in range(zn):
        swap(i).wait_send()
        if i < zn - 1:
            reduce_to(i).wait_send()
        if i > 0:
            spread(i).wait_send()
            reduce_out(i).wait_send()
            for n in range(2):
                aux(n, i).wait_send()

        def drain(d, _):
            forward(i, d).wait_send()
            swap_out(i, d).wait_send()
            return 0

        lax.fori_loop(0, sp, drain, 0)
        for d in range(1, sp):
            route(i, d).wait_send()
            back(i, d, s).wait_send()


def params(cid=None):
    if cid is None:
        return pltpu.CompilerParams(vmem_limit_bytes=VMEM_LIMIT)
    return pltpu.CompilerParams(
        collective_id=cid, has_side_effects=True, vmem_limit_bytes=VMEM_LIMIT
    )


def shards(
    tokens,
    query_vectors,
    key_vectors,
    value_vectors,
    cum_gate,
    out_weight,
    norm_gain,
    gate_weight,
    up_weight,
    down_weight,
    expert_ids,
    route_weights,
):
    sp = lax.axis_size("sp")
    tp = lax.axis_size("tp")
    zn = tp // 2
    seg, width = query_vectors.shape
    heads = cum_gate.shape[1]
    T, D = tokens.shape
    dma = pltpu.SemaphoreType.DMA

    n_experts = gate_weight.shape[0] * sp
    top = expert_ids.shape[1]
    cap = max(2, 3 * T * top // (2 * n_experts))
    cap = -(-cap // 8) * 8
    slots = n_experts * cap
    flat = expert_ids.reshape(-1)
    hits = (flat[:, None] == jnp.arange(n_experts, dtype=jnp.int32)[None, :]).astype(F32)
    lower = jnp.tril(jnp.ones((flat.shape[0], flat.shape[0]), F32), -1)
    earlier = jnp.dot(lower, hits, preferred_element_type=F32)
    slot = (flat * cap + jnp.sum(earlier * hits, axis=1).astype(jnp.int32)).reshape(T, top)
    match = slot[:, :, None] == jnp.arange(slots, dtype=jnp.int32)[None, None, :]
    place = jnp.any(match, axis=1).astype(BF16).T
    weight = jnp.sum(jnp.where(match, route_weights[:, :, None], 0.0), axis=1)
    high = lax.reduce_precision(weight, 8, 7)
    comb = jnp.concatenate([high, weight - high], axis=0).astype(BF16)

    fh = gate_weight.shape[2]
    partial = pl.pallas_call(
        functools.partial(attend_kernel, sp, heads),
        out_shape=jax.ShapeDtypeStruct((seg, D), BF16),
        in_specs=vmem_specs(5),
        out_specs=vmem_specs(1)[0],
        scratch_shapes=[
            pltpu.VMEM((sp, seg, width), BF16),
            pltpu.VMEM((sp, seg, width), BF16),
            pltpu.VMEM((sp, heads, seg), F32),
            pltpu.VMEM((seg, width), BF16),
            pltpu.VMEM((heads, seg, 1), F32),
            pltpu.VMEM((heads, seg, 1), F32),
            pltpu.VMEM((heads, seg, width // heads), F32),
            dma((3, sp)), dma((3, sp)),
        ],
        compiler_params=params(0),
        name="attend",
    )(query_vectors, key_vectors, value_vectors, cum_gate.T, out_weight)

    def vm(*shape, kind=BF16):
        return pltpu.VMEM(shape, kind)

    return pl.pallas_call(
        functools.partial(experts_kernel, sp, zn),
        out_shape=jax.ShapeDtypeStruct((T, D), BF16),
        in_specs=vmem_specs(5) + [pl.BlockSpec(memory_space=pl.ANY)] * 3,
        out_specs=vmem_specs(1)[0],
        scratch_shapes=[
            vm(D, fh), vm(D, fh), vm(fh, D),
            vm(zn, T, D), vm(zn, T, D), vm(zn, T, D), vm(zn, T, D),
            vm(zn, slots, T), vm(zn, 2 * T, slots),
            vm(zn, sp, cap, D),
            vm(zn, sp, 2, cap, D),
            vm(sp * 2 * cap, fh),
            vm(zn, sp, 2, cap, D),
            vm(zn, sp, cap, D), vm(zn, sp, cap, D), vm(zn, sp, cap, D),
            vm(zn, T, D), vm(zn, T, D),
            vm(T, D, kind=F32),
            dma((3,)),
            dma((zn,)), dma((zn,)),
            dma((2, zn)), dma((2, zn)),
            dma((zn,)), dma((zn,)),
            dma((zn,)), dma((zn,)),
            dma((zn, sp)), dma((zn, sp)),
            dma((zn, sp)), dma((zn, sp)),
            dma((zn, sp)), dma((zn, sp)),
            dma((zn, sp)), dma((zn, sp)),
            dma((zn,)), dma((zn,)),
        ],
        compiler_params=params(1),
        name="experts",
    )(partial, tokens, norm_gain[None, :], place, comb, gate_weight, up_weight, down_weight)


def solution(mesh):
    in_specs = (
        P(("sp", "tp"), None),
        P("sp", "tp"),
        P("sp", "tp"),
        P("sp", "tp"),
        P("sp", "tp"),
        P("tp", None),
        P(),
        P("sp", None, "tp"),
        P("sp", None, "tp"),
        P("sp", "tp", None),
        P(("sp", "tp"), None),
        P(("sp", "tp"), None),
    )
    out_specs = P(("sp", "tp"), None)
    return jax.shard_map(shards, mesh=mesh, in_specs=in_specs, out_specs=out_specs, check_vma=False)
```

profile of v0, /device:TPU:0, one launch (start us, length us, event | category | flops | bytes accessed | tf_op | source)
XLA Modules:
  0.0 173.8 jit_solution(16542616564450663522)
XLA Ops:
  0.0 0.8 copy.26
  0.8 0.1 eq.28
  0.9 0.2 fusion
  1.1 0.1 convert_element_type.18
  1.3 0.1 copy.27
  1.4 0.7 multiply_add_fusion
  2.1 0.1 fusion.1
  2.2 0.7 copy.28
  2.9 0.8 select_reduce_fusion
  3.7 0.6 pad_maximum_fusion.comb
  4.3 29.8 %attend.1.p = bf16[512,2048]{1,0:T(8,128)(2,1)} custom-call(bf16[512,256]{1,0:T(8,128)(2,1)} %q.1, bf16[512,256]{1,0:T(8,128)(2,1)} %k.1, bf16[512,256]{1,0:T(8,128)(2,1)} %v.1, f32[4,512]{1,0:T(4,128)} %bitcast.4, bf16[256,2048]{1,0:T(8,128)(2,1)} %w.1), custom_call_target="tpu_custom_call" | custom-call | tf_op jit(solution)/shard_map/attend/pallas_call | solution.py:397
  34.1 138.0 %experts.1 = bf16[64,2048]{1,0:T(8,128)(2,1)} custom-call(bf16[512,2048]{1,0:T(8,128)(2,1)} %attend.1.p, bf16[64,2048]{1,0:T(8,128)(2,1)} %tok.1, f32[1,2048]{1,0:T(1,128)} %bitcast.5, bf16[192,64]{1,0:T(8,128)(2,1)} %bitcast.3, bf16[128,192]{1,0:T(8,128)(2,1)} %pad_maximum_fusion.comb, bf16[1,2048,896]{2,1,0:T(8,128)(2,1)} %wg_in.1, ...), custom_call_target="tpu_custom_call" | custom-call | tf_op jit(solution)/shard_map/experts/pallas_call | solution.py:419
  172.1 1.7 copy.30
  (4 shorter events, 0.0 us)
where the time goes:
time: 174 us
  Pallas kernels  168 us (97%)
  local copies, waits for them, and re-layouts  3.5 us (2%)
  other arithmetic  2.24 us (1%)
    pallas_call x1, Pallas kernels, shards(): pl.pallas_call(functools.partial(experts_kernel, sp, zn), out_shape=jax.S...  138 us
    pallas_call x1, Pallas kernels, shards(): pl.pallas_call(functools.partial(attend_kernel, sp, heads), out_shape=jax...  29.8 us

commit v1 on v0

v1 whole, which is shorter than its diff:
```python
import functools
import math

import jax
import jax.numpy as jnp
from jax import lax
from jax.experimental import pallas as pl
from jax.experimental.pallas import tpu as pltpu
from jax.sharding import PartitionSpec as P

MESH = pl.DeviceIdType.MESH
VMEM_LIMIT = 60 * 1024 * 1024
F32 = jnp.float32
BF16 = jnp.bfloat16


def rcopy(src, dst, ssem, rsem, where):
    return pltpu.make_async_remote_copy(
        src_ref=src, dst_ref=dst, send_sem=ssem, recv_sem=rsem, device_id=where, device_id_type=MESH
    )


def vmem_specs(count):
    return [pl.BlockSpec(memory_space=pltpu.VMEM)] * count


def layer_kernel(
    sp, zn, heads, cap,
    q, k, v, g, tok, gain, ids, rw, w_in, wg_in, wu_in, wd_in, out,
    ka, va, ga, att, attp, top_s, sum_s, acc_s, wo, pf, sup, sdn, rup, rdn, ng,
    info, code, combs, wg, wu, wd, db, rows, hid, y, pr, cs, eb, mb, rr,
    ks, krs, ws, wxs, hs, as_, ars, us, urs, ns, nrs, ds_, drs, fs, frs, ps, prs, es, ers, ms, mrs,
):
    s, t = lax.axis_index("sp"), lax.axis_index("tp")
    z, c = lax.div(t, 2), lax.rem(t, 2)
    partner = t + 1 - 2 * c
    T, D = tok.shape
    seg, width = q.shape
    hd = width // heads
    loads = [
        pltpu.make_async_copy(a, b, ws.at[n])
        for n, (a, b) in enumerate(
            ((w_in, wo.at[0]), (wg_in.at[0], wg), (wu_in.at[0], wu), (wd_in.at[0], wd))
        )
    ]
    for load in loads:
        load.start()

    def at_z(zz):
        return {"tp": 2 * lax.rem(zz + zn, zn) + c}

    def peer(d):
        return lax.rem(s + d, sp)

    def behind(d):
        return lax.rem(s + sp - d, sp)

    barrier = pltpu.get_barrier_semaphore()
    pl.semaphore_signal(barrier, inc=1, device_id={"tp": partner}, device_id_type=MESH)
    for i in range(1, zn):
        pl.semaphore_signal(barrier, inc=1, device_id=at_z(z + i), device_id_type=MESH)
    for d in range(1, sp):
        pl.semaphore_signal(barrier, inc=1, device_id={"sp": peer(d)}, device_id_type=MESH)
    pl.semaphore_wait(barrier, 1 + (zn - 1) + (sp - 1))

    pairs = ((k, ka), (v, va), (g, ga))

    def share(n, d):
        src, dst = pairs[n]
        return rcopy(src, dst.at[d], ks.at[n, d], krs.at[n, d], {"sp": peer(d)})

    for d in range(1, sp):

        @pl.when(s + d < sp)
        def _():
            for n in range(3):
                share(n, d).start()

    weights = rcopy(w_in, wo.at[1], wxs.at[0], wxs.at[1], {"tp": partner})
    weights.start()

    many = info.shape[2]
    here = lax.broadcasted_iota(jnp.int32, (many, T), 0)
    hit = jnp.zeros((many, T), F32)
    wt = jnp.zeros((many, T), F32)
    for r in range(ids.shape[0]):
        same = ids[r : r + 1, :] == here
        hit = hit + jnp.where(same, 1.0, 0.0)
        wt = wt + jnp.where(same, rw[r : r + 1, :], 0.0)
    before = lax.broadcasted_iota(jnp.int32, (T, T), 0) < lax.broadcasted_iota(jnp.int32, (T, T), 1)
    rank = jnp.dot(
        hit.astype(BF16), jnp.where(before, 1.0, 0.0).astype(BF16), preferred_element_type=F32
    )
    info[z, 0] = jnp.where(hit > 0.5, rank, -1.0)
    info[z, 1] = wt

    def aux(i, origin):
        return rcopy(info.at[origin], info.at[origin], as_.at[i], ars.at[i], at_z(z + i))

    for i in range(1, zn):
        aux(i, z).start()

    tile = math.gcd(seg, 256)
    log2e = 1.4426950408889634
    coef = hd ** (-0.5) * log2e
    units = [(h, i) for h in range(heads) for i in range(seg // tile)]

    def scores(h, i, kb, gb):
        qt = q[i * tile : (i + 1) * tile, h * hd : (h + 1) * hd]
        return (
            lax.dot_general(qt, kb, (((1,), (1,)), ((), ())), preferred_element_type=F32) * coef
            - gb * log2e
        )

    for h, i in units:
        cols = slice(h * hd, (h + 1) * hd)
        seen = (i + 1) * tile
        sc = scores(h, i, k[0:seen, cols], g[h : h + 1, 0:seen])
        row = lax.broadcasted_iota(jnp.int32, sc.shape, 0) + i * tile
        col = lax.broadcasted_iota(jnp.int32, sc.shape, 1)
        sc = jnp.where(col <= row, sc, -1e30)
        peak = jnp.max(sc, axis=1, keepdims=True)
        ex = jnp.exp2(sc - peak)
        at = slice(i * tile, seen)
        top_s[h, at] = peak
        sum_s[h, at] = jnp.sum(ex, axis=1, keepdims=True)
        acc_s[h, at] = jnp.dot(ex.astype(BF16), v[0:seen, cols], preferred_element_type=F32)

    def step(d, _):
        for n in range(3):
            share(n, d).wait_recv()
        for h, i in units:
            cols = slice(h * hd, (h + 1) * hd)
            at = slice(i * tile, (i + 1) * tile)
            sc = scores(h, i, ka[d, :, cols], ga[d, h : h + 1, :])
            peak = top_s[h, at]
            new = jnp.maximum(peak, jnp.max(sc, axis=1, keepdims=True))
            ex = jnp.exp2(sc - new)
            fix = jnp.exp2(peak - new)
            top_s[h, at] = new
            sum_s[h, at] = sum_s[h, at] * fix + jnp.sum(ex, axis=1, keepdims=True)
            acc_s[h, at] = acc_s[h, at] * fix + jnp.dot(
                ex.astype(BF16), va[d, :, cols], preferred_element_type=F32
            )
        return 0

    lax.fori_loop(1, s + 1, step, 0)
    for h, i in units:
        for b in range(i * tile // T, (i + 1) * tile // T):
            at = slice(b * T, (b + 1) * T)
            att[b % 2, b // 2, :, h * hd : (h + 1) * hd] = (acc_s[h, at] / sum_s[h, at]).astype(BF16)
    heads_swap = rcopy(att.at[1 - c], attp, hs.at[0], hs.at[1], {"tp": partner})
    heads_swap.start()
    loads[0].wait()
    weights.wait_recv()
    heads_swap.wait_recv()

    halves = 2
    part = D // halves
    chunk = math.gcd(part, 512)
    mine = att[c].reshape(zn * T, width)
    other = attp[...].reshape(zn * T, width)

    def hop(up, dest, h):
        cut = slice(h * part, (h + 1) * part)
        src, dst = (sup, rup) if up else (sdn, rdn)
        return rcopy(
            src.at[dest, :, cut], dst.at[dest, :, cut], us.at[up, dest, h], urs.at[up, dest, h],
            at_z(z + 1 if up else z - 1),
        )

    def project(h):
        for n in range(part // chunk):
            cut = slice(h * part + n * chunk, h * part + (n + 1) * chunk)
            got = jnp.dot(mine, wo[0, :, cut], preferred_element_type=F32) + jnp.dot(
                other, wo[1, :, cut], preferred_element_type=F32
            )
            pf[:, :, cut] = got.reshape(zn, T, chunk)

    def push(kk, h):
        cut = slice(h * part, (h + 1) * part)
        for up in (1, 0):
            dest = zn - 1 - kk if up else kk
            going = z < dest if up else z > dest
            first = z == 0 if up else z == zn - 1
            inner = z > 0 if up else z < zn - 1
            src, dst = (sup, rup) if up else (sdn, rdn)

            @pl.when(jnp.logical_and(going, first))
            def _():
                src[dest, :, cut] = pf[dest, :, cut].astype(BF16)
                hop(up, dest, h).start()

            @pl.when(jnp.logical_and(going, inner))
            def _():
                hop(up, dest, h).wait_recv()
                src[dest, :, cut] = (pf[dest, :, cut] + dst[dest, :, cut].astype(F32)).astype(BF16)
                hop(up, dest, h).start()

    for h in range(halves):
        project(h)
        if h == 0:
            pass
    for kk in range(zn - 1):
        for h in range(halves):
            push(kk, h)
    for h in range(halves):
        cut = slice(h * part, (h + 1) * part)

        @pl.when(z > 0)
        def _():
            hop(1, z, h).wait_recv()
            pf[z, :, cut] = pf[z, :, cut] + rup[z, :, cut].astype(F32)

        @pl.when(z < zn - 1)
        def _():
            hop(0, z, h).wait_recv()
            pf[z, :, cut] = pf[z, :, cut] + rdn[z, :, cut].astype(F32)

    st = (tok[...].astype(F32) + pf[z]).astype(BF16)
    out[...] = st
    wide = st.astype(F32)
    inverse = lax.rsqrt(jnp.mean(wide * wide, axis=1, keepdims=True) + 1e-05)
    ng[z] = (wide * inverse * gain[...]).astype(BF16)

    high = lax.div(2 * z, zn)
    low_z = z + high * (zn - 1 - 2 * z)

    def origin(j):
        if j == 0:
            return z
        a = (j + 1) // 2
        near = lax.div(zn + low_z - a, zn)
        o = near * (low_z + (a if j % 2 == 0 else -a)) + (1 - near) * j
        return o + high * (zn - 1 - 2 * o)

    def along(o):
        up = lax.div(zn + z - o - 1, zn)
        far = up * (z - o) + (1 - up) * (o - z)
        return up, far

    def carry(o, up, far):
        ref = ng.at[o]
        return rcopy(ref, ref, ns.at[up, far], nrs.at[up, far], at_z(z + 2 * up - 1))

    def arrived(o, up, far):
        ref = ng.at[o]
        return rcopy(ref, ref, ns.at[up, far], nrs.at[up, far - 1], at_z(z))

    def onward(o, up, far, act):
        goes = z + 2 * up - 1

        @pl.when(jnp.logical_and(goes >= 0, goes < zn))
        def _():
            act(carry(o, up, far))

    def own_block(act):
        @pl.when(z < zn - 1)
        def _():
            act(carry(z, 1, 0))

        @pl.when(z > 0)
        def _():
            act(carry(z, 0, 0))

    own_block(lambda cp: cp.start())

    def route(j, d):
        return rcopy(
            db.at[j, peer(d)], rows.at[j, s, c], ds_.at[j, d], drs.at[j, d], {"sp": peer(d)}
        )

    def routed(j, d):
        return rcopy(
            db.at[j, peer(d)], rows.at[j, behind(d), c], ds_.at[j, d], drs.at[j, d], {"sp": peer(d)}
        )

    def forward(j, d):
        ref = rows.at[j, behind(d), c]
        return rcopy(ref, ref, fs.at[j, d], frs.at[j, d], {"tp": partner})

    def forwarded(j, d):
        ref = rows.at[j, behind(d), 1 - c]
        return rcopy(ref, ref, fs.at[j, d], frs.at[j, d], {"tp": partner})

    def swap_out(j, d):
        return rcopy(y.at[j, peer(d), 1 - c], pr.at[j, d], ps.at[j, d], prs.at[j, d], {"tp": partner})

    def back(j, d, slot):
        return rcopy(cs.at[j, d], eb.at[j, slot], es.at[j, d], ers.at[j, d], {"sp": peer(d)})

    def reduce_out(j):
        return rcopy(mb.at[j], rr.at[z], ms.at[j], mrs.at[z], at_z(origin(j)))

    def reduced(i):
        zz = lax.rem(z + i, zn)
        return rcopy(mb.at[0], rr.at[zz], ms.at[0], mrs.at[zz], at_z(z))

    def dispatch(j):
        o = origin(j)
        if j > 0:
            up, far = along(o)
            arrived(o, up, far).wait_recv()
            onward(o, up, far, lambda cp: cp.start())
            aux(lax.rem(z - o + zn, zn), o).wait_recv()
        spots = lax.broadcasted_iota(jnp.int32, (cap, T), 0).astype(F32)
        for e in range(sp):
            code[e * cap : (e + 1) * cap] = jnp.where(info[o, 0, e : e + 1, :] == spots, 1.0, 0.0)
        moved = jnp.dot(code[...].astype(BF16), ng[o], preferred_element_type=F32)
        for e in range(sp):
            db[j, e] = moved[e * cap : (e + 1) * cap].astype(BF16)
        for d in range(1, sp):
            route(j, d).start()
        rows[j, s, c] = db[j, s]
        forward(j, 0).start()
        for e in range(sp):
            code[e * cap : (e + 1) * cap] = jnp.where(
                info[o, 0, e : e + 1, :] == spots, jnp.broadcast_to(info[o, 1, e : e + 1, :], (cap, T)), 0.0
            )
        given = code[...]
        coarse = given.astype(BF16)
        combs[j, 0] = coarse
        combs[j, 1] = (given - coarse.astype(F32)).astype(BF16)

    def pass_on(j):
        def arrive(d, _):
            routed(j, d).wait_recv()
            forward(j, d).start()
            return 0

        lax.fori_loop(1, sp, arrive, 0)

    def each(count, body):
        if count * rows.shape[1] <= 64:
            for n in range(count):
                body(n)
        else:
            lax.fori_loop(0, count, lambda n, _: (body(n), 0)[1], 0)

    def expert(j):
        def landed(d, _):
            forwarded(j, d).wait_recv()
            return 0

        lax.fori_loop(0, sp, landed, 0)
        x = rows.at[j]
        many = sp * 2 * cap
        units = wg.shape[1]
        step = 256

        def into(start, size):
            cut = pl.ds(start, size)
            xv = x[...].reshape(many, D)
            gate = jnp.dot(xv, wg[:, cut], preferred_element_type=F32)
            up = jnp.dot(xv, wu[:, cut], preferred_element_type=F32)
            hid[:, cut] = (gate / (1.0 + jnp.exp(-gate)) * up).astype(BF16)

        each(units // step, lambda n: into(pl.multiple_of(n * step, step), step))
        if units % step:
            into(units - units % step, units % step)
        chunk = math.gcd(D, 512)

        def down(n):
            cut = pl.ds(pl.multiple_of(n * chunk, chunk), chunk)
            got = jnp.dot(hid[...], wd[:, cut], preferred_element_type=F32).astype(BF16)
            y[j, :, :, :, cut] = got.reshape(sp, 2, cap, chunk)

        each(D // chunk, down)
        for d in list(range(1, sp)) + [0]:
            swap_out(j, d).start()

    def give_back(j):
        def both(d):
            swap_out(j, d).wait_recv()
            return (y[j, peer(d), c].astype(F32) + pr[j, d].astype(F32)).astype(BF16)

        def send(d, _):
            cs[j, d] = both(d)
            back(j, d, s).start()
            return 0

        lax.fori_loop(1, sp, send, 0)
        eb[j, s] = both(0)

    def mix(j):
        for d in range(1, sp):
            back(j, d, behind(d)).wait_recv()
        ev = eb[j].reshape(sp * cap, D)
        dims = (((0,), (0,)), ((), ()))
        return lax.dot_general(combs[j, 0], ev, dims, preferred_element_type=F32) + lax.dot_general(
            combs[j, 1], ev, dims, preferred_element_type=F32
        )

    dispatch(0)
    if zn > 1:
        dispatch(1)
    for load in loads[1:]:
        load.wait()
    for j in range(zn):
        pass_on(j)
        if j + 2 < zn:
            dispatch(j + 2)
        expert(j)
        if j >= 2:
            give_back(j - 1)
    if zn > 1:
        give_back(zn - 1)
    give_back(0)
    for j in range(1, zn):
        mb[j] = mix(j).astype(BF16)
        reduce_out(j).start()
    total = out[...].astype(F32) + mix(0)
    for i in range(1, zn):
        reduced(i).wait_recv()
        total = total + rr[lax.rem(z + i, zn)].astype(F32)
    out[...] = total.astype(BF16)

    for d in range(1, sp):

        @pl.when(s + d < sp)
        def _():
            for n in range(3):
                share(n, d).wait_send()

    weights.wait_send()
    heads_swap.wait_send()
    own_block(lambda cp: cp.wait_send())
    for kk in range(zn - 1):
        for h in range(halves):
            for up in (1, 0):
                dest = zn - 1 - kk if up else kk

                @pl.when(z < dest if up else z > dest)
                def _():
                    hop(up, dest, h).wait_send()

    for j in range(zn):
        if j > 0:
            aux(j, z).wait_send()
            o = origin(j)
            onward(o, *along(o), lambda cp: cp.wait_send())
            reduce_out(j).wait_send()

        def drain(d, _):
            forward(j, d).wait_send()
            swap_out(j, d).wait_send()
            return 0

        lax.fori_loop(0, sp, drain, 0)
        for d in range(1, sp):
            route(j, d).wait_send()
            back(j, d, s).wait_send()


def shards(
    tokens,
    query_vectors,
    key_vectors,
    value_vectors,
    cum_gate,
    out_weight,
    norm_gain,
    gate_weight,
    up_weight,
    down_weight,
    expert_ids,
    route_weights,
):
    sp = lax.axis_size("sp")
    tp = lax.axis_size("tp")
    zn = tp // 2
    seg, width = query_vectors.shape
    heads = cum_gate.shape[1]
    T, D = tokens.shape
    dma = pltpu.SemaphoreType.DMA

    n_experts = gate_weight.shape[0] * sp
    top = expert_ids.shape[1]
    cap = max(2, 3 * T * top // (2 * n_experts))
    cap = -(-cap // 8) * 8
    slots = n_experts * cap
    kinds = -(-n_experts // 8) * 8
    fh = gate_weight.shape[2]

    def vm(*shape, kind=BF16):
        return pltpu.VMEM(shape, kind)

    return pl.pallas_call(
        functools.partial(layer_kernel, sp, zn, heads, cap),
        out_shape=jax.ShapeDtypeStruct((T, D), BF16),
        in_specs=vmem_specs(8) + [pl.BlockSpec(memory_space=pl.ANY)] * 4,
        out_specs=vmem_specs(1)[0],
        scratch_shapes=[
            vm(sp, seg, width), vm(sp, seg, width), vm(sp, heads, seg, kind=F32),
            vm(2, zn, T, width), vm(zn, T, width),
            vm(heads, seg, 1, kind=F32), vm(heads, seg, 1, kind=F32),
            vm(heads, seg, width // heads, kind=F32),
            vm(2, width, D), vm(zn, T, D, kind=F32),
            vm(zn, T, D), vm(zn, T, D), vm(zn, T, D), vm(zn, T, D), vm(zn, T, D),
            vm(zn, 2, kinds, T, kind=F32), vm(slots, T, kind=F32), vm(zn, 2, slots, T),
            vm(D, fh), vm(D, fh), vm(fh, D),
            vm(zn, sp, cap, D),
            vm(zn, sp, 2, cap, D),
            vm(sp * 2 * cap, fh),
            vm(zn, sp, 2, cap, D),
            vm(zn, sp, cap, D), vm(zn, sp, cap, D), vm(zn, sp, cap, D),
            vm(zn, T, D), vm(zn, T, D),
            dma((3, sp)), dma((3, sp)),
            dma((4,)), dma((2,)), dma((2,)),
            dma((zn,)), dma((zn,)),
            dma((2, zn, 2)), dma((2, zn, 2)),
            dma((2, zn)), dma((2, zn)),
            dma((zn, sp)), dma((zn, sp)),
            dma((zn, sp)), dma((zn, sp)),
            dma((zn, sp)), dma((zn, sp)),
            dma((zn, sp)), dma((zn, sp)),
            dma((zn,)), dma((zn,)),
        ],
        compiler_params=pltpu.CompilerParams(
            collective_id=0, has_side_effects=True, vmem_limit_bytes=VMEM_LIMIT
        ),
        name="layer",
    )(
        query_vectors, key_vectors, value_vectors, cum_gate.T, tokens, norm_gain[None, :],
        expert_ids.T, route_weights.T, out_weight, gate_weight, up_weight, down_weight,
    )


def solution(mesh):
    in_specs = (
        P(("sp", "tp"), None),
        P("sp", "tp"),
        P("sp", "tp"),
        P("sp", "tp"),
        P("sp", "tp"),
        P("tp", None),
        P(),
        P("sp", None, "tp"),
        P("sp", None, "tp"),
        P("sp", "tp", None),
        P(("sp", "tp"), None),
        P(("sp", "tp"), None),
    )
    out_specs = P(("sp", "tp"), None)
    return jax.shard_map(shards, mesh=mesh, in_specs=in_specs, out_specs=out_specs, check_vma=False)
```

time: 174 us -> 151 us (0.87)
  Pallas kernels: 168 us -> 149 us
  other arithmetic: 2.24 us -> 0 us
  local copies, waits for them, and re-layouts: 3.5 us -> 1.67 us
    pallas_call x2 -> x1, Pallas kernels: 168 us -> 149 us  [shards(): pl.pallas_call(functools.partial(layer_kernel, sp, zn, heads, cap), out_s...]
where the time goes in v1:
time: 151 us
  Pallas kernels  149 us (99%)
  local copies, waits for them, and re-layouts  1.67 us (1%)
    pallas_call x1, Pallas kernels, shards(): pl.pallas_call(functools.partial(layer_kernel, sp, zn, heads, cap), out_s...  149 us

profile of v1, /device:TPU:0, one launch (start us, length us, event | category | flops | bytes accessed | tf_op | source)
XLA Modules:
  0.0 151.1 jit_solution(4311070865167743170)
XLA Ops:
  0.0 149.5 %layer.1 = bf16[64,2048]{1,0:T(8,128)(2,1)} custom-call(bf16[512,256]{1,0:T(8,128)(2,1)} %q.1, bf16[512,256]{1,0:T(8,128)(2,1)} %k.1, bf16[512,256]{1,0:T(8,128)(2,1)} %v.1, f32[4,512]{1,0:T(4,128)} %bitcast.4, bf16[64,2048]{1,0:T(8,128)(2,1)} %tok.1, f32[1,2048]{1,0:T(1,128)} %bitcast.5, s32[2,64]{1,0:T(2,128)} %bitcast.6, f32[2,64]{1,0:T(2,128)} %bitcast.7, ...), custom_call_target="tpu_custom_call" | custom-call | tf_op jit(solution)/shard_map/layer/pallas_call | solution.py:488
  149.5 1.7 %copy.14 = bf16[64,2048]{1,0:T(8,128)(2,1)} copy(bf16[64,2048]{1,0:T(8,128)(2,1)} %layer.1) | data formatting | bytes 524288

commit v2 on v1

--- a/solution.py
+++ b/solution.py
@@ -29,7 +29,7 @@
     q, k, v, g, tok, gain, ids, rw, w_in, wg_in, wu_in, wd_in, out,
     ka, va, ga, att, attp, top_s, sum_s, acc_s, wo, pf, sup, sdn, rup, rdn, ng,
     info, code, combs, wg, wu, wd, db, rows, hid, y, pr, cs, eb, mb, rr,
-    ks, krs, ws, wxs, hs, as_, ars, us, urs, ns, nrs, ds_, drs, fs, frs, ps, prs, es, ers, ms, mrs,
+    ks, krs, kx, gs, ws, wxs, hs, as_, ars, us, urs, ns, nrs, ds_, drs, fs, frs, ps, prs, es, ers, ms, mrs,
 ):
     s, t = lax.axis_index("sp"), lax.axis_index("tp")
     z, c = lax.div(t, 2), lax.rem(t, 2)
@@ -63,18 +63,63 @@
         pl.semaphore_signal(barrier, inc=1, device_id={"sp": peer(d)}, device_id_type=MESH)
     pl.semaphore_wait(barrier, 1 + (zn - 1) + (sp - 1))
 
-    pairs = ((k, ka), (v, va), (g, ga))
-
-    def share(n, d):
+    pairs = ((k, ka), (v, va))
+    square = sp == 4 and heads % 2 == 0 and (width // 2) % 128 == 0
+    splits = 2 if square else 1
+    lanes = width // splits
+
+    def strip(f):
+        return slice(f * lanes, (f + 1) * lanes)
+
+    def share(n, f, d):
         src, dst = pairs[n]
-        return rcopy(src, dst.at[d], ks.at[n, d], krs.at[n, d], {"sp": peer(d)})
+        return rcopy(
+            src.at[:, strip(f)], dst.at[d, :, strip(f)], ks.at[n, f, d], krs.at[n, f, d], {"sp": peer(d)}
+        )
+
+    def share_gate(d):
+        return rcopy(g, ga.at[d], gs.at[0, d], gs.at[1, d], {"sp": peer(d)})
+
+    def pass_kv(n, f, d, to, slot):
+        dst = pairs[n][1]
+        return rcopy(
+            dst.at[d, :, strip(f)], dst.at[slot, :, strip(f)], kx.at[n, f], krs.at[n, f, slot],
+            {"sp": lax.rem(to + sp, sp)},
+        )
+
+    def sends(d):
+        if not square:
+            return s + d < sp
+        if d == 3:
+            return s > sp
+        return jnp.logical_and(s + d < sp, s != 1) if d == 1 else s + d < sp
+
+    def relays(f, d):
+        if not square:
+            return ()
+        corner = jnp.logical_and(s == 3, d == 2)
+        last = (s == 1) if f == 0 else jnp.logical_and(s == 2, d == 2)
+        return ((corner, s - 1, 1), (last, s + 2 - f, 3))
+
+    def share_all(cond, f, d):
+        @pl.when(cond)
+        def _():
+            for n in range(2):
+                share(n, f, d).start()
 
     for d in range(1, sp):
 
         @pl.when(s + d < sp)
         def _():
-            for n in range(3):
-                share(n, d).start()
+            share_gate(d).start()
+
+    for f in range(splits):
+        for d in range(1, sp):
+            if square and d == 2:
+                share_all(s == 1, f, d)
+                share_all(s == 0, 1 - f, d)
+            else:
+                share_all(sends(d), f, d)
 
     weights = rcopy(w_in, wo.at[1], wxs.at[0], wxs.at[1], {"tp": partner})
     weights.start()
@@ -104,6 +149,7 @@
     log2e = 1.4426950408889634
     coef = hd ** (-0.5) * log2e
     units = [(h, i) for h in range(heads) for i in range(seg // tile)]
+    each_split = heads // splits
 
     def scores(h, i, kb, gb):
         qt = q[i * tile : (i + 1) * tile, h * hd : (h + 1) * hd]
@@ -126,10 +172,19 @@
         sum_s[h, at] = jnp.sum(ex, axis=1, keepdims=True)
         acc_s[h, at] = jnp.dot(ex.astype(BF16), v[0:seen, cols], preferred_element_type=F32)
 
-    def step(d, _):
-        for n in range(3):
-            share(n, d).wait_recv()
+    def land(f, d):
+        for n in range(2):
+            share(n, f, d).wait_recv()
+            for cond, to, slot in relays(f, d):
+
+                @pl.when(cond)
+                def _():
+                    pass_kv(n, f, d, to, slot).start()
+
+    def absorb(f, d):
         for h, i in units:
+            if h // each_split != f:
+                continue
             cols = slice(h * hd, (h + 1) * hd)
             at = slice(i * tile, (i + 1) * tile)
             sc = scores(h, i, ka[d, :, cols], ga[d, h : h + 1, :])
@@ -142,6 +197,29 @@
             acc_s[h, at] = acc_s[h, at] * fix + jnp.dot(
                 ex.astype(BF16), va[d, :, cols], preferred_element_type=F32
             )
+
+    def step(i, _):
+        if not square:
+            share_gate(i).wait_recv()
+            land(0, i)
+            absorb(0, i)
+            return 0
+        d = jnp.where(i == 1, jnp.where(s == 1, 1, 2), jnp.where(i == 2, 1, 3))
+        early = jnp.logical_and(s == 2, d == 2)
+        share_gate(d).wait_recv()
+
+        @pl.when(early)
+        def _():
+            land(1, d)
+
+        land(0, d)
+        absorb(0, d)
+
+        @pl.when(jnp.logical_not(early))
+        def _():
+            land(1, d)
+
+        absorb(1, d)
         return 0
 
     lax.fori_loop(1, s + 1, step, 0)
@@ -177,11 +255,12 @@
             )
             pf[:, :, cut] = got.reshape(zn, T, chunk)
 
-    def push(kk, h):
+    def push(tau, h):
         cut = slice(h * part, (h + 1) * part)
         for up in (1, 0):
-            dest = zn - 1 - kk if up else kk
-            going = z < dest if up else z > dest
+            wave = tau - z if up else tau - (zn - 1 - z)
+            dest = zn - 1 - wave if up else wave
+            going = jnp.logical_and(wave >= 0, z < dest if up else z > dest)
             first = z == 0 if up else z == zn - 1
             inner = z > 0 if up else z < zn - 1
             src, dst = (sup, rup) if up else (sdn, rdn)
@@ -199,11 +278,9 @@
 
     for h in range(halves):
         project(h)
-        if h == 0:
-            pass
-    for kk in range(zn - 1):
+    for tau in range(zn - 1):
         for h in range(halves):
-            push(kk, h)
+            push(tau, h)
     for h in range(halves):
         cut = slice(h * part, (h + 1) * part)
 
@@ -402,11 +479,10 @@
             dispatch(j + 2)
         expert(j)
         if j >= 2:
-            give_back(j - 1)
-    if zn > 1:
-        give_back(zn - 1)
+            give_back(j)
+    give_back(1)
     give_back(0)
-    for j in range(1, zn):
+    for j in list(range(2, zn)) + [1]:
         mb[j] = mix(j).astype(BF16)
         reduce_out(j).start()
     total = out[...].astype(F32) + mix(0)
@@ -417,10 +493,23 @@
 
     for d in range(1, sp):
 
+        @pl.when(sends(d))
+        def _():
+            for n in range(2):
+                for f in range(splits):
+                    share(n, f, d).wait_send()
+
         @pl.when(s + d < sp)
         def _():
-            for n in range(3):
-                share(n, d).wait_send()
+            share_gate(d).wait_send()
+
+    for f in range(splits):
+        for cond, to, slot in ((s == 3, s - 1, 1), (s == (2 if f else 1), s + 2 - f, 3)) if square else ():
+
+            @pl.when(cond)
+            def _():
+                for n in range(2):
+                    pass_kv(n, f, 2, to, slot).wait_send()
 
     weights.wait_send()
     heads_swap.wait_send()
@@ -505,7 +594,7 @@
             vm(zn, sp, 2, cap, D),
             vm(zn, sp, cap, D), vm(zn, sp, cap, D), vm(zn, sp, cap, D),
             vm(zn, T, D), vm(zn, T, D),
-            dma((3, sp)), dma((3, sp)),
+            dma((2, 2, sp)), dma((2, 2, sp)), dma((2, 2)), dma((2, sp)),
             dma((4,)), dma((2,)), dma((2,)),
             dma((zn,)), dma((zn,)),
             dma((2, zn, 2)), dma((2, zn, 2)),

time: 151 us -> 134 us (0.89)
  Pallas kernels: 149 us -> 132 us
    pallas_call x1, Pallas kernels: 149 us -> 132 us  [shards(): pl.pallas_call(functools.partial(layer_kernel, sp, zn, heads, cap), out_s...]
where the time goes in v2:
time: 134 us
  Pallas kernels  132 us (99%)
  local copies, waits for them, and re-layouts  1.67 us (1%)
    pallas_call x1, Pallas kernels, shards(): pl.pallas_call(functools.partial(layer_kernel, sp, zn, heads, cap), out_s...  132 us

profile of v2, /device:TPU:0, one launch (start us, length us, event | category | flops | bytes accessed | tf_op | source)
XLA Modules:
  0.0 134.1 jit_solution(4981248657018933431)
XLA Ops:
  0.0 132.4 %layer.1 = bf16[64,2048]{1,0:T(8,128)(2,1)} custom-call(bf16[512,256]{1,0:T(8,128)(2,1)} %q.1, bf16[512,256]{1,0:T(8,128)(2,1)} %k.1, bf16[512,256]{1,0:T(8,128)(2,1)} %v.1, f32[4,512]{1,0:T(4,128)} %bitcast.4, bf16[64,2048]{1,0:T(8,128)(2,1)} %tok.1, f32[1,2048]{1,0:T(1,128)} %bitcast.5, s32[2,64]{1,0:T(2,128)} %bitcast.6, f32[2,64]{1,0:T(2,128)} %bitcast.7, ...), custom_call_target="tpu_custom_call" | custom-call | tf_op jit(solution)/shard_map/layer/pallas_call | solution.py:577
  132.4 1.7 %copy.14 = bf16[64,2048]{1,0:T(8,128)(2,1)} copy(bf16[64,2048]{1,0:T(8,128)(2,1)} %layer.1) | data formatting | bytes 524288

commit v3 on v2

--- a/solution.py
+++ b/solution.py
@@ -28,8 +28,8 @@
     sp, zn, heads, cap,
     q, k, v, g, tok, gain, ids, rw, w_in, wg_in, wu_in, wd_in, out,
     ka, va, ga, att, attp, top_s, sum_s, acc_s, wo, pf, sup, sdn, rup, rdn, ng,
-    info, code, combs, wg, wu, wd, db, rows, hid, y, pr, cs, eb, mb, rr,
-    ks, krs, kx, gs, ws, wxs, hs, as_, ars, us, urs, ns, nrs, ds_, drs, fs, frs, ps, prs, es, ers, ms, mrs,
+    info, code, combs, wg, wu, wd, db, rows, hid, y, pr, cs, eb, mb, rr, bs, zb,
+    ks, krs, kx, gs, ws, wxs, hs, as_, ars, us, urs, ns, nrs, ds_, drs, fs, frs, ps, prs, es, ers, ms, mrs, ffs, ffrs, zs, zrs, bfs, bfrs,
 ):
     s, t = lax.axis_index("sp"), lax.axis_index("tp")
     z, c = lax.div(t, 2), lax.rem(t, 2)
@@ -49,18 +49,26 @@
     def at_z(zz):
         return {"tp": 2 * lax.rem(zz + zn, zn) + c}
 
+    def ahead(d):
+        return lax.rem(s + d, sp)
+
+    bits = max(sp - 1, 1).bit_length()
+    paired = sp == 1 << bits
+
     def peer(d):
-        return lax.rem(s + d, sp)
+        if not paired:
+            return lax.rem(s + d, sp)
+        return sum(lax.rem(lax.div(s, 1 << b) + d // (1 << b), 2) * (1 << b) for b in range(bits))
 
     def behind(d):
-        return lax.rem(s + sp - d, sp)
+        return peer(d) if paired else lax.rem(s + sp - d, sp)
 
     barrier = pltpu.get_barrier_semaphore()
     pl.semaphore_signal(barrier, inc=1, device_id={"tp": partner}, device_id_type=MESH)
     for i in range(1, zn):
         pl.semaphore_signal(barrier, inc=1, device_id=at_z(z + i), device_id_type=MESH)
     for d in range(1, sp):
-        pl.semaphore_signal(barrier, inc=1, device_id={"sp": peer(d)}, device_id_type=MESH)
+        pl.semaphore_signal(barrier, inc=1, device_id={"sp": ahead(d)}, device_id_type=MESH)
     pl.semaphore_wait(barrier, 1 + (zn - 1) + (sp - 1))
 
     pairs = ((k, ka), (v, va))
@@ -74,11 +82,11 @@
     def share(n, f, d):
         src, dst = pairs[n]
         return rcopy(
-            src.at[:, strip(f)], dst.at[d, :, strip(f)], ks.at[n, f, d], krs.at[n, f, d], {"sp": peer(d)}
+            src.at[:, strip(f)], dst.at[d, :, strip(f)], ks.at[n, f, d], krs.at[n, f, d], {"sp": ahead(d)}
         )
 
     def share_gate(d):
-        return rcopy(g, ga.at[d], gs.at[0, d], gs.at[1, d], {"sp": peer(d)})
+        return rcopy(g, ga.at[d], gs.at[0, d], gs.at[1, d], {"sp": ahead(d)})
 
     def pass_kv(n, f, d, to, slot):
         dst = pairs[n][1]
@@ -316,79 +324,129 @@
         far = up * (z - o) + (1 - up) * (o - z)
         return up, far
 
-    def carry(o, up, far):
-        ref = ng.at[o]
-        return rcopy(ref, ref, ns.at[up, far], nrs.at[up, far], at_z(z + 2 * up - 1))
-
-    def arrived(o, up, far):
-        ref = ng.at[o]
-        return rcopy(ref, ref, ns.at[up, far], nrs.at[up, far - 1], at_z(z))
-
-    def onward(o, up, far, act):
+    in_z, out_z = D // 4, bs.shape[3]
+    first_in, rest_in = slice(0, in_z), slice(in_z, D)
+    first_out, rest_out = slice(0, out_z), slice(out_z, D)
+
+    def block(kind, o):
+        return rows.at[o, :, c, :, first_in] if kind else ng.at[o, :, rest_in]
+
+    def carry(kind, o, up, far):
+        ref = block(kind, o)
+        return rcopy(ref, ref, ns.at[kind, up, far], nrs.at[kind, up, far], at_z(z + 2 * up - 1))
+
+    def arrived(kind, o, up, far):
+        ref = block(kind, o)
+        return rcopy(ref, ref, ns.at[kind, up, far], nrs.at[kind, up, far - 1], at_z(z))
+
+    def onward(kind, o, up, far, act):
         goes = z + 2 * up - 1
 
         @pl.when(jnp.logical_and(goes >= 0, goes < zn))
         def _():
-            act(carry(o, up, far))
-
-    def own_block(act):
+            act(carry(kind, o, up, far))
+
+    def own_block(kind, act):
         @pl.when(z < zn - 1)
         def _():
-            act(carry(z, 1, 0))
+            act(carry(kind, z, 1, 0))
 
         @pl.when(z > 0)
         def _():
-            act(carry(z, 0, 0))
-
-    own_block(lambda cp: cp.start())
+            act(carry(kind, z, 0, 0))
+
+    own_block(0, lambda cp: cp.start())
+
+    def span(j):
+        return rest_in if j > 0 else slice(0, D)
 
     def route(j, d):
         return rcopy(
-            db.at[j, peer(d)], rows.at[j, s, c], ds_.at[j, d], drs.at[j, d], {"sp": peer(d)}
+            db.at[j, peer(d), :, span(j)], rows.at[origin(j), s, c, :, span(j)],
+            ds_.at[j, d], drs.at[j, d], {"sp": peer(d)},
         )
 
     def routed(j, d):
         return rcopy(
-            db.at[j, peer(d)], rows.at[j, behind(d), c], ds_.at[j, d], drs.at[j, d], {"sp": peer(d)}
+            db.at[j, peer(d), :, span(j)], rows.at[origin(j), behind(d), c, :, span(j)],
+            ds_.at[j, d], drs.at[j, d], {"sp": peer(d)},
         )
 
     def forward(j, d):
-        ref = rows.at[j, behind(d), c]
+        ref = rows.at[origin(j), behind(d), c, :, span(j)]
         return rcopy(ref, ref, fs.at[j, d], frs.at[j, d], {"tp": partner})
 
     def forwarded(j, d):
-        ref = rows.at[j, behind(d), 1 - c]
+        ref = rows.at[origin(j), behind(d), 1 - c, :, span(j)]
         return rcopy(ref, ref, fs.at[j, d], frs.at[j, d], {"tp": partner})
+
+    def forward_first(j, core):
+        ref = rows.at[origin(j), :, core, :, first_in]
+        return rcopy(ref, ref, ffs.at[j], ffrs.at[j], {"tp": partner})
 
     def swap_out(j, d):
         return rcopy(y.at[j, peer(d), 1 - c], pr.at[j, d], ps.at[j, d], prs.at[j, d], {"tp": partner})
 
     def back(j, d, slot):
-        return rcopy(cs.at[j, d], eb.at[j, slot], es.at[j, d], ers.at[j, d], {"sp": peer(d)})
+        return rcopy(
+            cs.at[j, d, :, rest_out], eb.at[j, slot, :, rest_out], es.at[j, d], ers.at[j, d],
+            {"sp": peer(d)},
+        )
+
+    def back_first(d, slot):
+        return rcopy(
+            cs.at[0, d, :, first_out], eb.at[0, slot, :, first_out], bfs.at[d], bfrs.at[d],
+            {"sp": peer(d)},
+        )
+
+    def home(j):
+        return rcopy(bs.at[j], zb.at[z], zs.at[j], zrs.at[z], at_z(origin(j)))
+
+    def homed(zz):
+        return rcopy(bs.at[0], zb.at[zz], zs.at[0], zrs.at[zz], at_z(z))
 
     def reduce_out(j):
-        return rcopy(mb.at[j], rr.at[z], ms.at[j], mrs.at[z], at_z(origin(j)))
+        return rcopy(
+            mb.at[j, :, rest_out], rr.at[z, :, rest_out], ms.at[j], mrs.at[z], at_z(origin(j))
+        )
 
     def reduced(i):
         zz = lax.rem(z + i, zn)
-        return rcopy(mb.at[0], rr.at[zz], ms.at[0], mrs.at[zz], at_z(z))
+        return rcopy(mb.at[0, :, rest_out], rr.at[zz, :, rest_out], ms.at[0], mrs.at[zz], at_z(z))
+
+    def relay(kind, j):
+        o = origin(j)
+        up, far = along(o)
+
+        def act(cp):
+            arrived(kind, o, up, far).wait_recv()
+            cp.start()
+
+        onward(kind, o, up, far, act)
+
+    def ended(kind, j):
+        o = origin(j)
+        up, far = along(o)
+        goes = z + 2 * up - 1
+
+        @pl.when(jnp.logical_or(goes < 0, goes >= zn))
+        def _():
+            arrived(kind, o, up, far).wait_recv()
 
     def dispatch(j):
         o = origin(j)
         if j > 0:
-            up, far = along(o)
-            arrived(o, up, far).wait_recv()
-            onward(o, up, far, lambda cp: cp.start())
+            ended(0, j)
             aux(lax.rem(z - o + zn, zn), o).wait_recv()
         spots = lax.broadcasted_iota(jnp.int32, (cap, T), 0).astype(F32)
         for e in range(sp):
             code[e * cap : (e + 1) * cap] = jnp.where(info[o, 0, e : e + 1, :] == spots, 1.0, 0.0)
-        moved = jnp.dot(code[...].astype(BF16), ng[o], preferred_element_type=F32)
+        moved = jnp.dot(code[...].astype(BF16), ng[o, :, span(j)], preferred_element_type=F32)
         for e in range(sp):
-            db[j, e] = moved[e * cap : (e + 1) * cap].astype(BF16)
-        for d in range(1, sp):
+            db[j, e, :, span(j)] = moved[e * cap : (e + 1) * cap].astype(BF16)
+        for d in range(sp - 1, 0, -1):
             route(j, d).start()
-        rows[j, s, c] = db[j, s]
+        rows[o, s, c, :, span(j)] = db[j, s, :, span(j)]
         forward(j, 0).start()
         for e in range(sp):
             code[e * cap : (e + 1) * cap] = jnp.where(
@@ -407,6 +465,10 @@
 
         lax.fori_loop(1, sp, arrive, 0)
 
+    def pass_first(j):
+        ended(1, j)
+        forward_first(j, c).start()
+
     def each(count, body):
         if count * rows.shape[1] <= 64:
             for n in range(count):
@@ -420,7 +482,9 @@
             return 0
 
         lax.fori_loop(0, sp, landed, 0)
-        x = rows.at[j]
+        if j > 0:
+            forward_first(j, 1 - c).wait_recv()
+        x = rows.at[origin(j)]
         many = sp * 2 * cap
         units = wg.shape[1]
         step = 256
@@ -443,53 +507,100 @@
             y[j, :, :, :, cut] = got.reshape(sp, 2, cap, chunk)
 
         each(D // chunk, down)
-        for d in list(range(1, sp)) + [0]:
+        for d in range(sp - 1, -1, -1):
             swap_out(j, d).start()
 
     def give_back(j):
-        def both(d):
+        def settle(d, ref):
             swap_out(j, d).wait_recv()
-            return (y[j, peer(d), c].astype(F32) + pr[j, d].astype(F32)).astype(BF16)
-
-        def send(d, _):
-            cs[j, d] = both(d)
+            got = y[j, peer(d), c].astype(F32) + pr[j, d].astype(F32)
+            ref[:, rest_out] = got[:, rest_out].astype(BF16)
+            if j > 0:
+                bs[j, d] = got[:, first_out].astype(BF16)
+
+        def send(n, _):
+            d = sp - n
+            settle(d, cs.at[j, d])
             back(j, d, s).start()
             return 0
 
         lax.fori_loop(1, sp, send, 0)
-        eb[j, s] = both(0)
-
-    def mix(j):
-        for d in range(1, sp):
-            back(j, d, behind(d)).wait_recv()
-        ev = eb[j].reshape(sp * cap, D)
+        settle(0, eb.at[j, s])
+        if j > 0:
+            home(j).start()
+
+    def give_first():
+        for i in range(1, zn):
+            homed(lax.rem(z + i, zn)).wait_recv()
+
+        def gather(d):
+            got = y[0, peer(d), c, :, first_out].astype(F32) + pr[0, d, :, first_out].astype(F32)
+            for i in range(1, zn):
+                got = got + zb[lax.rem(z + i, zn), d].astype(F32)
+            return got.astype(BF16)
+
+        def send(n, _):
+            d = sp - n
+            cs[0, d, :, first_out] = gather(d)
+            back_first(d, s).start()
+            return 0
+
+        lax.fori_loop(1, sp, send, 0)
+        eb[0, s, :, first_out] = gather(0)
+
+    def mix(j, cut):
+        ev = eb[j, :, :, cut].reshape(sp * cap, cut.stop - cut.start)
         dims = (((0,), (0,)), ((), ()))
         return lax.dot_general(combs[j, 0], ev, dims, preferred_element_type=F32) + lax.dot_general(
             combs[j, 1], ev, dims, preferred_element_type=F32
         )
 
+    def returned(j):
+        for d in range(sp - 1, 0, -1):
+            back(j, d, behind(d)).wait_recv()
+
+    def mix_out(j):
+        returned(j)
+        mb[j, :, rest_out] = mix(j, rest_out).astype(BF16)
+        reduce_out(j).start()
+
     dispatch(0)
-    if zn > 1:
-        dispatch(1)
+    relay(0, 1)
+    relay(0, 2)
+    dispatch(1)
     for load in loads[1:]:
         load.wait()
     for j in range(zn):
         pass_on(j)
-        if j + 2 < zn:
+        if j == 0:
+            dispatch(2)
+            for n in range(3, zn):
+                relay(0, n)
+            own_block(1, lambda cp: cp.start())
+        elif j + 2 < zn:
             dispatch(j + 2)
+        if j > 0:
+            if j == 1:
+                relay(1, 1)
+            if j + 1 < zn:
+                relay(1, j + 1)
+            pass_first(j)
         expert(j)
-        if j >= 2:
+        if j > 0:
             give_back(j)
-    give_back(1)
     give_back(0)
-    for j in list(range(2, zn)) + [1]:
-        mb[j] = mix(j).astype(BF16)
-        reduce_out(j).start()
-    total = out[...].astype(F32) + mix(0)
+    for j in range(1, zn):
+        mix_out(j)
+    give_first()
+    returned(0)
+    total = out[:, rest_out].astype(F32) + mix(0, rest_out)
     for i in range(1, zn):
         reduced(i).wait_recv()
-        total = total + rr[lax.rem(z + i, zn)].astype(F32)
-    out[...] = total.astype(BF16)
+        total = total + rr[lax.rem(z + i, zn), :, rest_out].astype(F32)
+    out[:, rest_out] = total.astype(BF16)
+    for d in range(1, sp):
+        back_first(d, behind(d)).wait_recv()
+    out[:, first_out] = (out[:, first_out].astype(F32) + mix(0, first_out)).astype(BF16)
 
     for d in range(1, sp):
 
@@ -513,7 +624,8 @@
 
     weights.wait_send()
     heads_swap.wait_send()
-    own_block(lambda cp: cp.wait_send())
+    for kind in (0, 1):
+        own_block(kind, lambda cp: cp.wait_send())
     for kk in range(zn - 1):
         for h in range(halves):
             for up in (1, 0):
@@ -527,8 +639,11 @@
         if j > 0:
             aux(j, z).wait_send()
             o = origin(j)
-            onward(o, *along(o), lambda cp: cp.wait_send())
+            for kind in (0, 1):
+                onward(kind, o, *along(o), lambda cp: cp.wait_send())
             reduce_out(j).wait_send()
+            home(j).wait_send()
+            forward_first(j, c).wait_send()
 
         def drain(d, _):
             forward(j, d).wait_send()
@@ -539,6 +654,8 @@
         for d in range(1, sp):
             route(j, d).wait_send()
             back(j, d, s).wait_send()
+            if j == 0:
+                back_first(d, s).wait_send()
 
 
 def shards(
@@ -594,16 +711,19 @@
             vm(zn, sp, 2, cap, D),
             vm(zn, sp, cap, D), vm(zn, sp, cap, D), vm(zn, sp, cap, D),
             vm(zn, T, D), vm(zn, T, D),
+            vm(zn, sp, cap, D // 8), vm(zn, sp, cap, D // 8),
             dma((2, 2, sp)), dma((2, 2, sp)), dma((2, 2)), dma((2, sp)),
             dma((4,)), dma((2,)), dma((2,)),
             dma((zn,)), dma((zn,)),
             dma((2, zn, 2)), dma((2, zn, 2)),
-            dma((2, zn)), dma((2, zn)),
+            dma((2, 2, zn)), dma((2, 2, zn)),
             dma((zn, sp)), dma((zn, sp)),
             dma((zn, sp)), dma((zn, sp)),
             dma((zn, sp)), dma((zn, sp)),
             dma((zn, sp)), dma((zn, sp)),
             dma((zn,)), dma((zn,)),
+            dma((zn,)), dma((zn,)), dma((zn,)), dma((zn,)),
+            dma((sp,)), dma((sp,)),
         ],
         compiler_params=pltpu.CompilerParams(
             collective_id=0, has_side_effects=True, vmem_limit_bytes=VMEM_LIMIT

time: 134 us -> 127 us (0.948)
  Pallas kernels: 132 us -> 124 us
    pallas_call x1, Pallas kernels: 132 us -> 124 us  [shards(): pl.pallas_call(functools.partial(layer_kernel, sp, zn, heads, cap), out_s...]
where the time goes in v3:
time: 127 us; the launch traced here: 126 us
  Pallas kernels  124 us (98%)
  local copies, waits for them, and re-layouts  1.67 us (1%)
    pallas_call x1, Pallas kernels, shards(): pl.pallas_call(functools.partial(layer_kernel, sp, zn, heads, cap), out_s...  124 us

profile of v3, /device:TPU:0, one launch (start us, length us, event | category | flops | bytes accessed | tf_op | source)
XLA Modules:
  0.0 126.0 jit_solution(5032207398035460410)
XLA Ops:
  0.0 124.3 %layer.1 = bf16[64,2048]{1,0:T(8,128)(2,1)} custom-call(bf16[512,256]{1,0:T(8,128)(2,1)} %q.1, bf16[512,256]{1,0:T(8,128)(2,1)} %k.1, bf16[512,256]{1,0:T(8,128)(2,1)} %v.1, f32[4,512]{1,0:T(4,128)} %bitcast.4, bf16[64,2048]{1,0:T(8,128)(2,1)} %tok.1, f32[1,2048]{1,0:T(1,128)} %bitcast.5, s32[2,64]{1,0:T(2,128)} %bitcast.6, f32[2,64]{1,0:T(2,128)} %bitcast.7, ...), custom_call_target="tpu_custom_call" | custom-call | tf_op jit(solution)/shard_map/layer/pallas_call | solution.py:694
  124.3 1.7 %copy.14 = bf16[64,2048]{1,0:T(8,128)(2,1)} copy(bf16[64,2048]{1,0:T(8,128)(2,1)} %layer.1) | data formatting | bytes 524288
